TPU v7x, 32 devices: a whole 2x2x4 slice. The times are simulated.
32 devices in a mesh: fs: 8 (over z, y), tp: 4 (over x, core).
Axes of the slice: x: 2, y: 2, z: 4, core: 2. Of those that a mesh axis runs over, the one named last changes fastest.
Arguments:
- tokens: bfloat16 [3072, 2048], P('fs'), may hold values from -6 to 6
- first_norm_scale: float32 [2048], replicated, may hold values from 0.1 to 1.9
- recurrent_branch_matrix: bfloat16 [2048, 1024], P('fs', 'tp'), may hold values from -0.125 to 0.125
- gelu_gate_matrix: bfloat16 [2048, 1024], P('fs', 'tp'), may hold values from -0.125 to 0.125
- filter_taps_weight: bfloat16 [4, 1024], P(None, 'tp'), may hold values from -3 to 3
- recurrence_gate_blocks: bfloat16 [16, 64, 64], P('tp'), may hold values from -0.75 to 0.75
- input_gate_blocks: bfloat16 [16, 64, 64], P('tp'), may hold values from -0.75 to 0.75
- base_decay_logits: float32 [1024], P('tp'), may hold values from 4 to 11
- extra_log_decay: float32 [3072, 1024], P('fs', 'tp'), may hold values from -0.7 to 0
- mixer_output_matrix: bfloat16 [2048, 1024], P('fs', 'tp'), may hold values from -0.5 to 0.5
- second_norm_scale: float32 [2048], replicated, may hold values from 0.1 to 1.9
- mixer_up_matrix: bfloat16 [2048, 4096], P('fs', 'tp'), may hold values from -0.125 to 0.125
- mixer_down_matrix: bfloat16 [2048, 4096], P('fs', 'tp'), may hold values from -0.09375 to 0.09375
Outputs:
- layer_out: bfloat16 [3072, 2048], P(('fs', 'tp'))
All inputs are finite; a program needn't handle non-finite values.
Results may differ from a plain program's by a relative error of at most 0.022.
Values may be sent and summed in bfloat16 or wider, within the bound.
A program may use at most 64 MiB of HBM per device.

v0:
```python
import jax
import jax.numpy as jnp
from jax import lax
from jax.sharding import PartitionSpec as P

epsilon = 1e-06
decay_rate_scale = 8.0


def rms_scaled(sequence_token_rows, scales):
    widened = sequence_token_rows.astype(jnp.float32)
    mean_square = jnp.mean(widened * widened, axis=-1, keepdims=True)
    return (widened * lax.rsqrt(mean_square + epsilon) * scales).astype(jnp.bfloat16)


def linear_combine(earlier, later):
    return (earlier[0] * later[0], later[0] * earlier[1] + later[1])


def causal_taps(branch, filter_taps_weight):
    tap_count = filter_taps_weight.shape[0]
    positions = branch.shape[0]
    padded = jnp.pad(branch.astype(jnp.float32), ((tap_count - 1, 0), (0, 0)))
    running = jnp.zeros(branch.shape, jnp.float32)
    for offset in range(tap_count):
        running = running + padded[offset : offset + positions] * filter_taps_weight[offset].astype(
            jnp.float32
        )
    return running.astype(jnp.bfloat16)


def block_map(convolved, blocks):
    positions, channels = convolved.shape
    grouped = convolved.reshape(positions, blocks.shape[0], blocks.shape[1])
    mapped = jnp.einsum("sgi,gij->sgj", grouped, blocks, preferred_element_type=jnp.float32)
    return jax.nn.sigmoid(mapped.reshape(positions, channels))


def contract_columns(left, right):
    return lax.dot_general(
        left, right, (((1,), (1,)), ((), ())), preferred_element_type=jnp.float32
    )


def local(
    tokens,
    first_norm_scale,
    recurrent_branch_matrix,
    gelu_gate_matrix,
    filter_taps_weight,
    recurrence_gate_blocks,
    input_gate_blocks,
    base_decay_logits,
    extra_log_decay,
    mixer_output_matrix,
    second_norm_scale,
    mixer_up_matrix,
    mixer_down_matrix,
):
    positions = tokens.shape[0]
    own_count = positions // lax.axis_size("tp")
    normed = rms_scaled(tokens, first_norm_scale)
    branch_sum = jnp.dot(
        normed,
        lax.all_gather(recurrent_branch_matrix, "fs", axis=0, tiled=True),
        preferred_element_type=jnp.float32,
    )
    gate_sum = jnp.dot(
        normed,
        lax.all_gather(gelu_gate_matrix, "fs", axis=0, tiled=True),
        preferred_element_type=jnp.float32,
    )
    branch = branch_sum.astype(jnp.bfloat16)
    gate_branch = gate_sum.astype(jnp.bfloat16)
    out_full = lax.all_gather(mixer_output_matrix, "fs", axis=0, tiled=True)
    convolved = causal_taps(branch, filter_taps_weight)
    recurrence_gate_value = block_map(convolved, recurrence_gate_blocks)
    admission = block_map(convolved, input_gate_blocks)
    log_keep_factor = (
        decay_rate_scale * recurrence_gate_value * jax.nn.log_sigmoid(base_decay_logits)
        + extra_log_decay
    )
    retain = jnp.exp(log_keep_factor)
    driven = jnp.sqrt(-jnp.expm1(2.0 * log_keep_factor)) * (
        admission * convolved.astype(jnp.float32)
    )
    memory = lax.associative_scan(linear_combine, (retain, driven), axis=0)[1]
    recurrent = (memory * jax.nn.gelu(gate_branch.astype(jnp.float32))).astype(jnp.bfloat16)
    up_full = lax.all_gather(mixer_up_matrix, "fs", axis=0, tiled=True)
    whole_sum = lax.psum(contract_columns(recurrent, out_full).astype(jnp.bfloat16), "tp").astype(
        jnp.float32
    )
    residual_all = (tokens.astype(jnp.float32) + whole_sum).astype(jnp.bfloat16)
    raised = jnp.dot(
        rms_scaled(residual_all, second_norm_scale), up_full, preferred_element_type=jnp.float32
    )
    hidden = jnp.square(jax.nn.relu(raised)).astype(jnp.bfloat16)
    residual = lax.dynamic_slice_in_dim(
        residual_all, lax.axis_index("tp") * own_count, own_count, 0
    )
    down_full = lax.all_gather(mixer_down_matrix, "fs", axis=0, tiled=True)
    channel_sum = lax.psum_scatter(
        contract_columns(hidden, down_full).astype(jnp.bfloat16),
        "tp",
        scatter_dimension=0,
        tiled=True,
    ).astype(jnp.float32)
    return (residual.astype(jnp.float32) + channel_sum).astype(jnp.bfloat16)


def solution(mesh):
    in_specs = (
        P("fs", None),
        P(),
        P("fs", "tp"),
        P("fs", "tp"),
        P(None, "tp"),
        P("tp", None, None),
        P("tp", None, None),
        P("tp"),
        P("fs", "tp"),
        P("fs", "tp"),
        P(),
        P("fs", "tp"),
        P("fs", "tp"),
    )
    out_specs = P(("fs", "tp"), None)
    return jax.shard_map(local, mesh=mesh, in_specs=in_specs, out_specs=out_specs, check_vma=False)
```

profile of v0, /device:TPU:0, one launch (start us, length us, event | category | flops | bytes accessed | tf_op | source)
XLA Modules:
  0.0 372.9 jit_solution(10167174261476025850)
XLA Ops:
  6.5 0.7 all-gather.6.cloned.1.call-update
  7.3 0.0 all-gather.10.cloned.1.call-start
  7.3 0.7 all-gather.10.cloned.1.call-update
  8.0 0.0 all-gather.8.cloned.1.call-start
  8.1 0.7 all-gather.8.cloned.1.call-update
  8.7 0.0 all-reduce.19.cloned.1.call-start
  8.8 0.8 slice_convert_fusion.3
  9.6 1.8 fusion.3
  11.4 0.7 fusion.59
  12.1 40.4 %all-gather.6.cloned.1.call-done = bf16[2048,256]{1,0:T(8,128)(2,1)} async-done(((bf16[256,256]{1,0:T(8,128)(2,1)}), bf16[2048,256]{1,0:T(8,128)(2,1)}) %all-gather.6.cloned.1.call-update) | async-done | bytes 1048592 | tf_op jit(solution)/shard_map/all_gather | solution.py:65
  52.5 2.3 fusion.20
  54.8 0.0 copy-start.2
  54.9 0.2 add_convert_fusion.1
  55.0 0.2 copy.20
  55.2 0.3 fusion.18
  55.5 0.2 copy.22
  55.7 0.3 fusion.15
  56.0 0.2 copy.24
  56.2 0.5 fusion.49
  56.7 0.1 slice.221
  56.8 0.1 slice.222
  57.0 0.1 slice.220
  57.1 0.1 slice.224
  57.2 0.1 fusion.66
  58.3 0.3 slice.278
  58.6 0.3 slice.219
  59.1 0.0 copy-start.1
  59.1 0.0 copy-start.4
  59.6 0.1 pad.69
  59.7 0.1 fusion.44
  59.7 0.1 pad.68
  59.8 33.8 %all-gather.10.cloned.1.call-done = bf16[2048,256]{1,0:T(8,128)(2,1)} async-done(((bf16[256,256]{1,0:T(8,128)(2,1)}), bf16[2048,256]{1,0:T(8,128)(2,1)}) %all-gather.10.cloned.1.call-update) | async-done | bytes 1048592 | tf_op jit(solution)/shard_map/all_gather | solution.py:75
  93.6 41.2 %all-gather.8.cloned.1.call-done = bf16[2048,256]{1,0:T(8,128)(2,1)} async-done(((bf16[256,256]{1,0:T(8,128)(2,1)}), bf16[2048,256]{1,0:T(8,128)(2,1)}) %all-gather.8.cloned.1.call-update) | async-done | bytes 1048592 | tf_op jit(solution)/shard_map/all_gather | solution.py:70
  134.8 4.6 %convolution_convert_fusion.1 = bf16[384,2048]{1,0:T(8,128)(2,1)} fusion(bf16[2048,256]{1,0:T(8,128)(2,1)} %all-gather.10.cloned.1.call-done, bf16[2048,256]{1,0:T(8,128)(2,1)} %all-gather.8.cloned.1.call-done, bf16[384,2048]{1,0:T(8,128)(2,1)S(1)} %copy-done.1, f32[2048]{0:T(1024)S(1)} %copy-done.4, f32[384]{0:T(512)S(1)} %add_rsqrt_fusion.1, ...), kind=kOutput, calls=%fused_computation.13 | convolution fusion | flops 810516480 | bytes 6039040 | tf_op jit(solution)/shard_map/dot_general | solution.py:40
  139.4 0.0 all-reduce.19.cloned.1.call-update
  139.5 0.0 all-gather.12.cloned.1.call-start
  139.5 0.5 all-gather.12.cloned.1.call-update
  140.1 0.0 all-gather.14.cloned.1.call-start
  140.1 0.5 all-gather.14.cloned.1.call-update
  140.6 0.0 reduce-scatter.2.cloned.1.call-start
  140.7 40.5 %all-reduce.19.cloned.1.call-done = bf16[384,2048]{1,0:T(8,128)(2,1)} async-done(((bf16[384,2048]{1,0:T(8,128)(2,1)}), bf16[384,2048]{1,0:T(8,128)(2,1)}) %all-reduce.19.cloned.1.call-update) | async-done | bytes 1572880 | tf_op jit(solution)/shard_map/psum | solution.py:90
  181.2 2.1 fusion
  183.3 72.7 %all-gather.12.cloned.1.call-done = bf16[2048,1024]{1,0:T(8,128)(2,1)} async-done(((bf16[256,1024]{1,0:T(8,128)(2,1)}), bf16[2048,1024]{1,0:T(8,128)(2,1)}) %all-gather.12.cloned.1.call-update) | async-done | bytes 4194320 | tf_op jit(solution)/shard_map/all_gather | solution.py:89
  256.0 73.3 %all-gather.14.cloned.1.call-done = bf16[2048,1024]{1,0:T(8,128)(2,1)} async-done(((bf16[256,1024]{1,0:T(8,128)(2,1)}), bf16[2048,1024]{1,0:T(8,128)(2,1)}) %all-gather.14.cloned.1.call-update) | async-done | bytes 4194320 | tf_op jit(solution)/shard_map/all_gather | solution.py:101
  329.4 8.1 %convolution_convert_fusion = bf16[384,2048]{1,0:T(8,128)(2,1)} fusion(bf16[2048,1024]{1,0:T(8,128)(2,1)} %all-gather.14.cloned.1.call-done, bf16[2048,1024]{1,0:T(8,128)(2,1)} %all-gather.12.cloned.1.call-done, bf16[384,2048]{1,0:T(8,128)(2,1)S(1)} %get-tuple-element.6, f32[2048]{0:T(1024)S(1)} %copy-done.5, f32[384]{0:T(512)S(1)} %add_rsqrt_fusion), kind=kOutput, calls=%fused_computation.12 | convolution fusion | flops 3226337280 | bytes 11544064 | tf_op jit(solution)/shard_map/dot_general | solution.py:40
  337.5 0.0 reduce-scatter.2.cloned.1.call-update
  337.6 26.7 %reduce-scatter.2.cloned.1.call-done = bf16[96,2048]{1,0:T(8,128)(2,1)} async-done(((bf16[384,2048]{1,0:T(8,128)(2,1)}), bf16[96,2048]{1,0:T(8,128)(2,1)}) %reduce-scatter.2.cloned.1.call-update) | async-done | bytes 393232 | tf_op jit(solution)/shard_map/reduce_scatter | solution.py:102
  364.2 1.8 add_convert_fusion
  (96 shorter events, 1.3 us)
Async XLA Ops:
  6.5 48.7 %copy-start = (bf16[4,64,64]{2,1,0:T(8,128)(2,1)S(1)}, bf16[4,64,64]{2,1,0:T(8,128)(2,1)}, u32[]{:S(2)}) copy-start(bf16[4,64,64]{2,1,0:T(8,128)(2,1)} %param.18) | copy-start | bytes 98308
  6.5 46.0 %all-gather.6.cloned.1.call-start = ((), (), s32[]{:S(2)}) async-start(), calls=%async_computation.1 | async-start | bytes 1179648 | tf_op jit(solution)/shard_map/all_gather | solution.py:65
  7.3 86.4 %all-gather.10.cloned.1.call-start = ((), (), s32[]{:S(2)}) async-start(), calls=%async_computation.3 | async-start | bytes 1179648 | tf_op jit(solution)/shard_map/all_gather | solution.py:75
  8.0 126.8 %all-gather.8.cloned.1.call-start = ((), (), s32[]{:S(2)}) async-start(), calls=%async_computation.2 | async-start | bytes 1179648 | tf_op jit(solution)/shard_map/all_gather | solution.py:70
  8.7 172.4 %all-reduce.19.cloned.1.call-start = ((), (), s32[]{:S(2)}) async-start(), calls=%async_computation.4 | async-start | bytes 3145728 | tf_op jit(solution)/shard_map/psum | solution.py:90
  12.1 43.6 %copy-start.3 = (bf16[4,64,64]{2,1,0:T(8,128)(2,1)S(1)}, bf16[4,64,64]{2,1,0:T(8,128)(2,1)}, u32[]{:S(2)}) copy-start(bf16[4,64,64]{2,1,0:T(8,128)(2,1)} %param.19) | copy-start | bytes 98308
  54.8 1.4 copy-start.2
  59.1 75.7 %copy-start.1 = (bf16[384,2048]{1,0:T(8,128)(2,1)S(1)}, bf16[384,2048]{1,0:T(8,128)(2,1)}, u32[]{:S(2)}) copy-start(bf16[384,2048]{1,0:T(8,128)(2,1)} %param.13) | copy-start | bytes 4718596
  59.1 75.7 %copy-start.4 = (f32[2048]{0:T(1024)S(1)}, f32[2048]{0:T(1024)}, u32[]{:S(2)}) copy-start(f32[2048]{0:T(1024)} %param.14) | copy-start | bytes 24580
  139.5 189.9 %copy-start.5 = (f32[2048]{0:T(1024)S(1)}, f32[2048]{0:T(1024)}, u32[]{:S(2)}) copy-start(f32[2048]{0:T(1024)} %param.23) | copy-start | bytes 24580
  139.5 116.6 %all-gather.12.cloned.1.call-start = ((), (), s32[]{:S(2)}) async-start(), calls=%async_computation.5 | async-start | bytes 4718592 | tf_op jit(solution)/shard_map/all_gather | solution.py:89
  140.1 189.3 %all-gather.14.cloned.1.call-start = ((), (), s32[]{:S(2)}) async-start(), calls=%async_computation.6 | async-start | bytes 4718592 | tf_op jit(solution)/shard_map/all_gather | solution.py:101
  140.6 223.6 %reduce-scatter.2.cloned.1.call-start = ((), (), s32[]{:S(2)}) async-start(), calls=%async_computation.7 | async-start | bytes 1966080 | tf_op jit(solution)/shard_map/reduce_scatter | solution.py:102
Sparse Core Ops, SparseCore 0:
  9.5 42.9 all-gather.5
  54.6 38.9 all-gather.9
  95.8 38.9 all-gather.7
  139.6 41.5 all-reduce.18
  183.2 72.8 all-gather.11
  258.0 71.3 all-gather.13
  337.7 26.5 reduce-scatter.1
where the time goes:
time: 373 us
  waiting for transfers between devices  332 us (89%)
  matrix products  15.7 us (4%)
  between operations  14.1 us (4%)
  other arithmetic  8.42 us (2%)
    all_gather x1, waiting for transfers between devices, local(): down_full = lax.all_gather(mixer_down_matrix, 'fs', axis=0, tiled=True)  73.3 us
    all_gather x1, waiting for transfers between devices, local(): up_full = lax.all_gather(mixer_up_matrix, 'fs', axis=0, tiled=True)  72.7 us
    all_gather x1, waiting for transfers between devices, local(): lax.all_gather(gelu_gate_matrix, 'fs', axis=0, tiled=True)  41.2 us
    psum x1, waiting for transfers between devices, local(): lax.psum(contract_columns(recurrent, out_full).astype(jnp.bfloat16), 'tp')  40.5 us
    all_gather x1, waiting for transfers between devices, local(): lax.all_gather(recurrent_branch_matrix, 'fs', axis=0, tiled=True)  40.4 us
    all_gather x1, waiting for transfers between devices, local(): out_full = lax.all_gather(mixer_output_matrix, 'fs', axis=0, tiled=True)  33.8 us
    reduce_scatter x1, waiting for transfers between devices, local(): lax.psum_scatter(contract_columns(hidden, down_full).astype(jnp.bfloat16)...  26.7 us
    dot_general x2, matrix products, contract_columns(): lax.dot_general(left, right, (((1,), (1,)), ((), ())), preferred_element_...  12.8 us
  transfers between devices with their start and end apart: 7, of which 7 were waited for; matrix products, arithmetic and copies ran while one was open for 3% of the time, Pallas kernels for 0%

commit v1 on v0

--- a/solution.py
+++ b/solution.py
@@ -72,7 +72,6 @@
     )
     branch = branch_sum.astype(jnp.bfloat16)
     gate_branch = gate_sum.astype(jnp.bfloat16)
-    out_full = lax.all_gather(mixer_output_matrix, "fs", axis=0, tiled=True)
     convolved = causal_taps(branch, filter_taps_weight)
     recurrence_gate_value = block_map(convolved, recurrence_gate_blocks)
     admission = block_map(convolved, input_gate_blocks)
@@ -86,7 +85,16 @@
     )
     memory = lax.associative_scan(linear_combine, (retain, driven), axis=0)[1]
     recurrent = (memory * jax.nn.gelu(gate_branch.astype(jnp.float32))).astype(jnp.bfloat16)
-    up_full = lax.all_gather(mixer_up_matrix, "fs", axis=0, tiled=True)
+    out_full, up_full = jnp.split(
+        lax.all_gather(
+            jnp.concatenate([mixer_output_matrix, mixer_up_matrix], axis=1),
+            "fs",
+            axis=0,
+            tiled=True,
+        ),
+        [mixer_output_matrix.shape[1]],
+        axis=1,
+    )
     whole_sum = lax.psum(contract_columns(recurrent, out_full).astype(jnp.bfloat16), "tp").astype(
         jnp.float32
     )

time: 373 us -> 345 us (0.925)
  waiting for transfers between devices: 332 us -> 302 us
    all_gather x2 -> x1, waiting for transfers between devices: 107 us -> 86.8 us  [local(): lax.all_gather(jnp.concatenate([mixer_output_matrix, mixer_up_matrix], ax...]
    all_gather x1, waiting for transfers between devices: 41.2 us -> 31 us  [local(): lax.all_gather(gelu_gate_matrix, 'fs', axis=0, tiled=True)]
  transfers between devices with their start and end apart: 7 -> 6, of which waited for: 7 -> 6; matrix products, arithmetic and copies ran while one was open for 3% -> 4% of each run, Pallas kernels for 0% -> 0%
where the time goes in v1:
time: 345 us
  waiting for transfers between devices  302 us (88%)
  matrix products  15.1 us (4%)
  between operations  14.1 us (4%)
  other arithmetic  9.5 us (3%)
  local copies, waits for them, and re-layouts  4.06 us (1%)
    all_gather x1, waiting for transfers between devices, local(): lax.all_gather(jnp.concatenate([mixer_output_matrix, mixer_up_matrix], ax...  86.8 us
    all_gather x1, waiting for transfers between devices, local(): down_full = lax.all_gather(mixer_down_matrix, 'fs', axis=0, tiled=True)  72.7 us
    all_gather x1, waiting for transfers between devices, local(): lax.all_gather(recurrent_branch_matrix, 'fs', axis=0, tiled=True)  41.9 us
    psum x1, waiting for transfers between devices, local(): lax.psum(contract_columns(recurrent, out_full).astype(jnp.bfloat16), 'tp')  40.6 us
    all_gather x1, waiting for transfers between devices, local(): lax.all_gather(gelu_gate_matrix, 'fs', axis=0, tiled=True)  31 us
    reduce_scatter x1, waiting for transfers between devices, local(): lax.psum_scatter(contract_columns(hidden, down_full).astype(jnp.bfloat16)...  26.7 us
    dot_general x2, matrix products, contract_columns(): lax.dot_general(left, right, (((1,), (1,)), ((), ())), preferred_element_...  12.6 us
  transfers between devices with their start and end apart: 6, of which 6 were waited for; matrix products, arithmetic and copies ran while one was open for 4% of the time, Pallas kernels for 0%

profile of v1, /device:TPU:0, one launch (start us, length us, event | category | flops | bytes accessed | tf_op | source)
XLA Modules:
  0.0 344.6 jit_solution(11411139586150388234)
XLA Ops:
  6.5 0.0 copy-start
  6.5 0.0 all-gather.5.cloned.1.call-start
  6.6 0.7 all-gather.5.cloned.1.call-update
  7.3 0.0 all-gather.7.cloned.1.call-start
  7.3 0.7 all-gather.7.cloned.1.call-update
  8.0 0.0 all-gather.9.cloned.1.call-start
  8.1 2.0 pad_maximum_fusion
  10.0 0.0 all-gather.9.cloned.1.call-update
  10.1 0.0 all-reduce.19.cloned.1.call-start
  10.1 0.0 copy-done.1
  10.1 0.4 fusion.5
  10.5 0.0 copy-done.3
  10.6 0.0 copy-done.2
  10.6 0.0 copy-start.4
  10.6 41.9 %all-gather.5.cloned.1.call-done = bf16[2048,256]{1,0:T(8,128)(2,1)} async-done(((bf16[256,256]{1,0:T(8,128)(2,1)}), bf16[2048,256]{1,0:T(8,128)(2,1)}) %all-gather.5.cloned.1.call-update) | async-done | bytes 1048592 | tf_op jit(solution)/shard_map/all_gather | solution.py:65
  52.5 1.8 fusion.23
  54.4 0.2 add_convert_fusion.1
  54.6 0.2 copy.20
  54.7 0.3 fusion.21
  55.0 0.2 copy.22
  55.2 0.3 fusion.18
  55.5 0.9 copy.24
  56.5 1.6 fusion.56
  58.0 0.1 slice.221
  58.2 0.1 slice.222
  58.3 0.1 slice.220
  58.5 0.7 slice.224
  59.2 1.0 fusion.73
  61.2 0.3 slice.278
  61.5 0.3 slice.219
  62.5 0.1 pad.69
  62.5 0.1 fusion.51
  62.6 0.1 pad.68
  62.7 31.0 %all-gather.7.cloned.1.call-done = bf16[2048,256]{1,0:T(8,128)(2,1)} async-done(((bf16[256,256]{1,0:T(8,128)(2,1)}), bf16[2048,256]{1,0:T(8,128)(2,1)}) %all-gather.7.cloned.1.call-update) | async-done | bytes 1048592 | tf_op jit(solution)/shard_map/all_gather | solution.py:70
  93.7 86.8 %all-gather.9.cloned.1.call-done = bf16[2048,1280]{1,0:T(8,128)(2,1)} async-done(((bf16[256,1280]{1,0:T(8,128)(2,1)}), bf16[2048,1280]{1,0:T(8,128)(2,1)}) %all-gather.9.cloned.1.call-update) | async-done | bytes 5242896 | tf_op jit(solution)/shard_map/all_gather | solution.py:89
  180.5 4.6 %convolution_convert_fusion.1 = bf16[384,2048]{1,0:T(8,128)(2,1)} fusion(bf16[2048,1280]{1,0:T(8,128)(2,1)} %all-gather.9.cloned.1.call-done, bf16[2048,256]{1,0:T(8,128)(2,1)} %all-gather.7.cloned.1.call-done, bf16[384,2048]{1,0:T(8,128)(2,1)S(1)} %copy-done.1, f32[2048]{0:T(1024)S(1)} %copy-done.5, f32[384]{0:T(512)S(1)} %add_rsqrt_fusion.1, ...), kind=kOutput, calls=%fused_computation.15 | convolution fusion | flops 810516480 | bytes 6039040 | tf_op jit(solution)/shard_map/dot_general | solution.py:40
  185.1 0.0 all-reduce.19.cloned.1.call-update
  185.1 0.0 all-gather.11.cloned.1.call-start
  185.1 0.5 all-gather.11.cloned.1.call-update
  185.7 0.0 reduce-scatter.2.cloned.1.call-start
  185.7 40.6 %all-reduce.19.cloned.1.call-done = bf16[384,2048]{1,0:T(8,128)(2,1)} async-done(((bf16[384,2048]{1,0:T(8,128)(2,1)}), bf16[384,2048]{1,0:T(8,128)(2,1)}) %all-reduce.19.cloned.1.call-update) | async-done | bytes 1572880 | tf_op jit(solution)/shard_map/psum | solution.py:98
  226.3 2.1 fusion.2
  228.4 72.7 %all-gather.11.cloned.1.call-done = bf16[2048,1024]{1,0:T(8,128)(2,1)} async-done(((bf16[256,1024]{1,0:T(8,128)(2,1)}), bf16[2048,1024]{1,0:T(8,128)(2,1)}) %all-gather.11.cloned.1.call-update) | async-done | bytes 4194320 | tf_op jit(solution)/shard_map/all_gather | solution.py:109
  301.1 0.0 copy-done.6
  301.1 8.1 %convolution_convert_fusion = bf16[384,2048]{1,0:T(8,128)(2,1)} fusion(bf16[2048,1024]{1,0:T(8,128)(2,1)} %all-gather.11.cloned.1.call-done, bf16[2048,1280]{1,0:T(8,128)(2,1)} %all-gather.9.cloned.1.call-done, bf16[384,2048]{1,0:T(8,128)(2,1)S(1)} %get-tuple-element.6, f32[2048]{0:T(1024)S(1)} %copy-done.6, f32[384]{0:T(512)S(1)} %add_rsqrt_fusion), kind=kOutput, calls=%fused_computation.14 | convolution fusion | flops 3226337280 | bytes 11544064 | tf_op jit(solution)/shard_map/dot_general | solution.py:40
  309.2 0.0 reduce-scatter.2.cloned.1.call-update
  309.2 26.7 %reduce-scatter.2.cloned.1.call-done = bf16[96,2048]{1,0:T(8,128)(2,1)} async-done(((bf16[384,2048]{1,0:T(8,128)(2,1)}), bf16[96,2048]{1,0:T(8,128)(2,1)}) %reduce-scatter.2.cloned.1.call-update) | async-done | bytes 393232 | tf_op jit(solution)/shard_map/reduce_scatter | solution.py:110
  335.9 1.8 add_convert_fusion
  (96 shorter events, 1.3 us)
Async XLA Ops:
  6.5 48.2 %copy-start = (bf16[4,64,64]{2,1,0:T(8,128)(2,1)S(1)}, bf16[4,64,64]{2,1,0:T(8,128)(2,1)}, u32[]{:S(2)}) copy-start(bf16[4,64,64]{2,1,0:T(8,128)(2,1)} %param.18) | copy-start | bytes 98308
  6.5 3.6 %copy-start.1 = (bf16[384,2048]{1,0:T(8,128)(2,1)S(1)}, bf16[384,2048]{1,0:T(8,128)(2,1)}, u32[]{:S(2)}) copy-start(bf16[384,2048]{1,0:T(8,128)(2,1)} %param.13) | copy-start | bytes 4718596
  6.5 4.0 %copy-start.3 = (f32[256]{0:T(256)S(1)}, f32[256]{0:T(256)}, u32[]{:S(2)}) copy-start(f32[256]{0:T(256)} %param.20) | copy-start | bytes 3076
  6.5 4.0 %copy-start.2 = (bf16[4,256]{1,0:T(4,128)(2,1)S(1)}, bf16[4,256]{1,0:T(4,128)(2,1)}, u32[]{:S(2)}) copy-start(bf16[4,256]{1,0:T(4,128)(2,1)} %param.17) | copy-start | bytes 6148
  6.5 46.0 %copy-start.5 = (f32[2048]{0:T(1024)S(1)}, f32[2048]{0:T(1024)}, u32[]{:S(2)}) copy-start(f32[2048]{0:T(1024)} %param.14) | copy-start | bytes 24580
  6.5 46.0 %all-gather.5.cloned.1.call-start = ((), (), s32[]{:S(2)}) async-start(), calls=%async_computation.1 | async-start | bytes 1179648 | tf_op jit(solution)/shard_map/all_gather | solution.py:65
  7.3 86.4 %all-gather.7.cloned.1.call-start = ((), (), s32[]{:S(2)}) async-start(), calls=%async_computation.2 | async-start | bytes 1179648 | tf_op jit(solution)/shard_map/all_gather | solution.py:70
  8.0 172.4 %all-gather.9.cloned.1.call-start = ((), (), s32[]{:S(2)}) async-start(), calls=%async_computation.3 | async-start | bytes 5898240 | tf_op jit(solution)/shard_map/all_gather | solution.py:89
  10.1 216.2 %all-reduce.19.cloned.1.call-start = ((), (), s32[]{:S(2)}) async-start(), calls=%async_computation.4 | async-start | bytes 3145728 | tf_op jit(solution)/shard_map/psum | solution.py:98
  10.6 44.6 %copy-start.4 = (bf16[4,64,64]{2,1,0:T(8,128)(2,1)S(1)}, bf16[4,64,64]{2,1,0:T(8,128)(2,1)}, u32[]{:S(2)}) copy-start(bf16[4,64,64]{2,1,0:T(8,128)(2,1)} %param.19) | copy-start | bytes 98308
  185.1 116.1 %copy-start.6 = (f32[2048]{0:T(1024)S(1)}, f32[2048]{0:T(1024)}, u32[]{:S(2)}) copy-start(f32[2048]{0:T(1024)} %param.23) | copy-start | bytes 24580
  185.1 116.1 %all-gather.11.cloned.1.call-start = ((), (), s32[]{:S(2)}) async-start(), calls=%async_computation.5 | async-start | bytes 4718592 | tf_op jit(solution)/shard_map/all_gather | solution.py:109
  185.7 150.3 %reduce-scatter.2.cloned.1.call-start = ((), (), s32[]{:S(2)}) async-start(), calls=%async_computation.6 | async-start | bytes 1966080 | tf_op jit(solution)/shard_map/reduce_scatter | solution.py:110
Sparse Core Ops, SparseCore 0:
  9.5 42.9 all-gather.4
  54.6 38.9 all-gather.6
  95.9 84.5 all-gather.8
  185.2 41.0 all-reduce.18
  228.3 72.8 all-gather.10
  309.4 26.5 reduce-scatter.1
